TPU v7x, 32 devices: a whole 2x2x4 slice. The times are simulated.
32 devices in a mesh: sp: 16 (over z, y, x), tp: 2 (over core).
Axes of the slice: x: 2, y: 2, z: 4, core: 2. Of those that a mesh axis runs over, the one named last changes fastest.
Arguments:
- tokens: bfloat16 [4096, 2048], P('sp', 'tp'), may hold values from -6 to 6
- norm_gain: float32 [2048], replicated, may hold values from 0.1 to 1.9
- recur_query: bfloat16 [2048, 1024], P(None, 'tp'), may hold values from -0.125 to 0.125
- recur_forget: bfloat16 [2048, 1024], P(None, 'tp'), may hold values from -0.125 to 0.125
- recur_value: bfloat16 [2048, 1024], P(None, 'tp'), may hold values from -0.125 to 0.125
- gate_floor: float32 [1024], P('tp'), may hold values from 0.5 to 1
- extra_decay: float32 [4096, 8], P('sp', 'tp'), may hold values from 0 to 2
- start_state: float32 [8, 128, 128], P('tp'), may hold values from -0.125 to 0.125
- recur_gain: float32 [1024], P('tp'), may hold values from 0.1 to 1.9
- attend_query: bfloat16 [2048, 1024], P(None, 'tp')
- attend_key: bfloat16 [2048, 1024], P(None, 'tp')
- attend_value: bfloat16 [2048, 1024], P(None, 'tp'), may hold values from -0.125 to 0.125
- gate_cache: float32 [4096, 16], P(None, 'tp'), may hold values from -4096 to 0, as said below
- attend_gain: float32 [1024], P('tp'), may hold values from 0.1 to 1.9
- recur_output: bfloat16 [1024, 2048], P(None, 'tp'), may hold values from -0.1875 to 0.1875
- attend_output: bfloat16 [1024, 2048], P(None, 'tp'), may hold values from -0.1875 to 0.1875
Outputs:
- layer_output: bfloat16 [4096, 2048], P('sp', 'tp')
Inputs may be any that keep to these rules, and one draw needn't show every extreme that they name: `gate_cache`: never rising along positions.
All inputs are finite; a program needn't handle non-finite values.
Results may differ from a plain program's by a relative error of at most 0.018.
Values may be sent and summed in bfloat16 or wider, within the bound.
A program may use at most 64 MiB of HBM per device.

v0:
```python
import jax
import jax.numpy as jnp
from jax import lax
from jax.sharding import PartitionSpec as P

FD = 64
EPSILON = 1e-06
TOP_PRECISION = lax.Precision.HIGHEST


def prefix(x, axis, combine, identity):
    devices, position = (lax.axis_size(axis), lax.axis_index(axis))
    everything = jax.tree.map(
        lambda part, kind: lax.all_gather(part.astype(kind), axis), x, (jnp.bfloat16, jnp.bfloat16)
    )
    start = jax.tree.map(
        lambda part, zero: jnp.broadcast_to(jnp.asarray(zero, part.dtype), part.shape), x, identity
    )

    def step(k, before):
        reached = k < position
        new = combine(
            before, jax.tree.map(lambda part, own: part[k].astype(own.dtype), everything, x)
        )
        return jax.tree.map(lambda a, b: jnp.where(reached, a, b), new, before)

    return lax.fori_loop(0, devices, step, start)


def head_norm(per_head, head_gain):
    normed = per_head * lax.rsqrt(jnp.mean(per_head * per_head, axis=-1, keepdims=True) + EPSILON)
    return normed.reshape(per_head.shape[0], -1) * head_gain


def local_recurrence(query_rows, decays, inflow, values):
    span_len = min(64, query_rows.shape[0])
    blocks = query_rows.shape[0] // span_len

    def to_blocks(tensor):
        return tensor.reshape(blocks, span_len, tensor.shape[1], tensor.shape[2])

    causal = jnp.tril(jnp.ones((span_len, span_len), dtype=bool))[:, :, None, None]

    def advance(carried_state, pieces):
        query_block, g_block, k_block, value_block = pieces
        running_total = jnp.cumsum(g_block, axis=0)
        offsets = jnp.where(causal, running_total[:, None] - running_total[None, :], -jnp.inf)
        mixing = jnp.einsum(
            "thk,shk,tshk->hts", query_block, k_block, jnp.exp(offsets), precision=TOP_PRECISION
        )
        final_result = jnp.einsum("hts,shv->thv", mixing, value_block, precision=TOP_PRECISION)
        final_result = final_result + jnp.einsum(
            "dzc,zcu->dzu",
            query_block * jnp.exp(running_total),
            carried_state,
            precision=TOP_PRECISION,
        )
        ending_state = running_total[-1]
        weighted_values = k_block * jnp.exp(ending_state[None] - running_total)
        carried_state = jnp.exp(ending_state)[..., None] * carried_state + jnp.einsum(
            "cun,cub->unb", weighted_values, value_block, precision=TOP_PRECISION
        )
        return (carried_state, final_result)

    initial = jnp.zeros((query_rows.shape[1], query_rows.shape[2], values.shape[2]), jnp.float32)
    final_state, results = lax.scan(
        advance,
        initial,
        (to_blocks(query_rows), to_blocks(decays), to_blocks(inflow), to_blocks(values)),
    )
    return (results.reshape(query_rows.shape[0], query_rows.shape[1], values.shape[2]), final_state)


def keep_state(running_state):
    return running_state


def block_update(
    group_query, group_gates, group_index, key_rows, value_rows, key_gates, key_index, scaling
):

    def compute(running_state):
        maxima, totals, summed = running_state
        scores = (
            jnp.einsum("qhd,khd->hqk", group_query, key_rows, preferred_element_type=jnp.float32)
            * scaling
        )
        scores = scores + group_gates.T[:, :, None] - key_gates.T[:, None, :]
        allowed = (key_index[None, :] <= group_index[:, None])[None]
        highest = jnp.maximum(maxima, jnp.max(jnp.where(allowed, scores, -1e30), axis=-1))
        weights = jnp.where(allowed, jnp.exp(scores - highest[..., None]), 0.0)
        rescale = jnp.exp(maxima - highest)
        totals = totals * rescale + jnp.sum(weights, axis=-1)
        summed = summed * rescale.T[:, :, None] + jnp.einsum(
            "hqk,khd->qhd",
            weights.astype(jnp.bfloat16),
            value_rows,
            preferred_element_type=jnp.float32,
        )
        return (highest, totals, summed)

    return compute


def shards(
    tokens,
    norm_gain,
    recur_query,
    recur_forget,
    recur_value,
    gate_floor,
    extra_decay,
    start_state,
    recur_gain,
    attend_query,
    attend_key,
    attend_value,
    gate_cache,
    attend_gain,
    recur_output,
    attend_output,
):
    height = tokens.shape[0]
    model_width = norm_gain.shape[0]
    inputs = (recur_query, recur_forget, recur_value, attend_query, attend_key, attend_value)
    wide = lax.all_gather(tokens, "tp", axis=1, tiled=True).astype(jnp.float32)
    scaled = (wide * norm_gain).astype(jnp.bfloat16)
    updated = tuple(
        (jnp.dot(scaled, weight, preferred_element_type=jnp.float32) for weight in inputs)
    )
    products = updated
    squares = jnp.sum(wide * wide, axis=1, keepdims=True)
    inverse = lax.rsqrt(squares / model_width + EPSILON)
    projected = tuple(
        ((partial_value * inverse).astype(jnp.bfloat16) for partial_value in products)
    )
    rec_heads = start_state.shape[0]
    query_rows = projected[0].astype(jnp.float32).reshape(height, rec_heads, -1)
    forget_pre = projected[1].astype(jnp.float32).reshape(height, rec_heads, -1)
    values = projected[2].astype(jnp.float32).reshape(height, rec_heads, -1)
    inflow = (1.0 - gate_floor.reshape(rec_heads, -1)) * jax.nn.sigmoid(-forget_pre)
    decays = jnp.log1p(-inflow) - extra_decay[:, :, None]
    local_out, final_state = local_recurrence(query_rows, decays, inflow, values)
    running_total = jnp.cumsum(decays, axis=0)
    overall = running_total[-1]

    def compose(earlier, latter):
        return (earlier[0] * latter[0], latter[0][..., None] * earlier[1] + latter[1])

    identity = (jnp.ones_like(overall), jnp.zeros_like(final_state))
    passed, arriving = prefix((jnp.exp(overall), final_state), "sp", compose, identity)
    incoming_rows = passed[..., None] * start_state + arriving
    carried_out = jnp.einsum(
        "dzc,zcu->dzu", query_rows * jnp.exp(running_total), incoming_rows, precision=TOP_PRECISION
    )
    rec_rows = head_norm(local_out + carried_out, recur_gain).astype(jnp.bfloat16)
    att_heads = gate_cache.shape[1]
    att_query = projected[3].reshape(height, att_heads, FD)
    offset = lax.axis_index("sp") * height
    scaling = FD ** (-0.5)
    groups = ((att_query, offset, height),)
    prepared = tuple(
        (
            (
                group_query,
                lax.dynamic_slice_in_dim(gate_cache, group_start, rows, 0),
                group_start + jnp.arange(rows),
            )
            for group_query, group_start, rows in groups
        )
    )
    initial = tuple(
        (
            (
                jnp.full((att_heads, rows), -1e30, jnp.float32),
                jnp.zeros((att_heads, rows), jnp.float32),
                jnp.zeros((rows, att_heads, FD), jnp.float32),
            )
            for _, _, rows in groups
        )
    )
    key_part = lax.all_gather(projected[4], "sp", axis=0, tiled=True)
    value_part = lax.all_gather(projected[5], "sp", axis=0, tiled=True)
    total_amount = key_part.shape[0]
    step_rows = 2 * height

    def advance_keys(number, states):
        begin_at = number * step_rows
        key_rows = lax.dynamic_slice_in_dim(key_part, begin_at, step_rows, 0).reshape(
            step_rows, att_heads, FD
        )
        value_rows = lax.dynamic_slice_in_dim(value_part, begin_at, step_rows, 0).reshape(
            step_rows, att_heads, FD
        )
        key_gates = lax.dynamic_slice_in_dim(gate_cache, begin_at, step_rows, 0)
        key_index = begin_at + jnp.arange(step_rows)
        updated = []
        for (group_query, group_gates, group_index), state in zip(prepared, states):
            compute = block_update(
                group_query,
                group_gates,
                group_index,
                key_rows,
                value_rows,
                key_gates,
                key_index,
                scaling,
            )
            needed = begin_at <= group_index[-1]
            updated.append(lax.cond(needed, compute, keep_state, state))
        return tuple(updated)

    folded = lax.fori_loop(0, total_amount // step_rows, advance_keys, initial)
    row_parts = [
        head_norm(summed / totals.T[:, :, None], attend_gain).astype(jnp.bfloat16)
        for maxima, totals, summed in folded
    ]
    att_rows = row_parts[0]
    rec_all, att_all = (
        lax.all_gather(rec_rows, "tp", axis=1, tiled=True),
        lax.all_gather(att_rows, "tp", axis=1, tiled=True),
    )
    layer_sum = jnp.dot(rec_all, recur_output, preferred_element_type=jnp.float32)
    layer_sum = layer_sum + jnp.dot(att_all, attend_output, preferred_element_type=jnp.float32)
    return layer_sum.astype(jnp.bfloat16)


def solution(mesh):
    return jax.shard_map(
        shards,
        mesh=mesh,
        in_specs=(
            P("sp", "tp"),
            P(),
            P(None, "tp"),
            P(None, "tp"),
            P(None, "tp"),
            P("tp"),
            P("sp", "tp"),
            P("tp", None, None),
            P("tp"),
            P(None, "tp"),
            P(None, "tp"),
            P(None, "tp"),
            P(None, "tp"),
            P("tp"),
            P(None, "tp"),
            P(None, "tp"),
        ),
        out_specs=P("sp", "tp"),
        check_vma=False,
    )
```

profile of v0, /device:TPU:29, one launch (start us, length us, event | category | flops | bytes accessed | tf_op | source)
XLA Modules:
  0.0 403.0 jit_solution(830316774274925419)
XLA Ops:
  8.8 10.8 %all-gather.6.cloned.1.call-done = bf16[256,2048]{1,0:T(8,128)(2,1)} async-done(((bf16[256,1024]{1,0:T(8,128)(2,1)}), bf16[256,2048]{1,0:T(8,128)(2,1)}) %all-gather.6.cloned.1.call-update) | async-done | bytes 1048592 | tf_op jit(solution)/shard_map/all_gather | solution.py:126
  21.1 2.7 fusion.51
  28.5 2.6 fusion.46
  33.8 76.5 %while.47 = (s32[]{:T(128)}, f32[4,128,128]{2,1,0:T(8,128)S(1)}, f32[4,64,4,128]{3,1,0,2:T(8,128)}, f32[4,64,4,128]{3,2,1,0:T(4,128)}, f32[4,64,4,128]{3,2,1,0:T...) while((s32[]{:T(128)}, f32[4,128,128]{2,1,0:T(8,128)S(1)}, ...), condition=%wide.region_3.4_spmd.clone, body=%wide.region_1.3_spmd.clone.sunk | while | flops 138760192 | bytes 21254276 | solution.py:66
  34.8 5.9 %exponential_bitcast_fusion.2 = f32[4,64,64,128]{3,0,2,1:T(4,128)S(1)} fusion(f32[64,4,128]{2,1,0:T(4,128)S(1)} %fusion.102, pred[64,64]{1,0:T(8,128)(4,1)S(1)} %fusion.104), kind=kLoop, calls=%fused_computation.29.clone.1 | loop fusion | flops 4194304 | bytes 8523776 | tf_op jit(solution)/shard_map/while
  41.6 7.3 %fusion.105 = f32[4,64,64]{1,2,0:T(8,128)S(1)} fusion(f32[4,64,64,128]{3,0,2,1:T(4,128)S(1)} %exponential_bitcast_fusion.2, f32[4,128,64]{1,2,0:T(8,128)S(1)} %copy.154, f32[4,128,64]{1,2,0:T(8,128)S(1)} %copy.155), kind=kLoop, calls=%fused_computation.28.clone.1 | loop fusion | flops 6275072 | bytes 8716288 | tf_op jit(solution)/shard_map/while/body/eval_jaxpr/thk,shk,tshk->hts/dot_general | solution.py:48
  53.9 5.9 %exponential_bitcast_fusion.2 = f32[4,64,64,128]{3,0,2,1:T(4,128)S(1)} fusion(f32[64,4,128]{2,1,0:T(4,128)S(1)} %fusion.102, pred[64,64]{1,0:T(8,128)(4,1)S(1)} %fusion.104), kind=kLoop, calls=%fused_computation.29.clone.1 | loop fusion | flops 4194304 | bytes 8523776 | tf_op jit(solution)/shard_map/while
  60.8 7.3 %fusion.105 = f32[4,64,64]{1,2,0:T(8,128)S(1)} fusion(f32[4,64,64,128]{3,0,2,1:T(4,128)S(1)} %exponential_bitcast_fusion.2, f32[4,128,64]{1,2,0:T(8,128)S(1)} %copy.154, f32[4,128,64]{1,2,0:T(8,128)S(1)} %copy.155), kind=kLoop, calls=%fused_computation.28.clone.1 | loop fusion | flops 6275072 | bytes 8716288 | tf_op jit(solution)/shard_map/while/body/eval_jaxpr/thk,shk,tshk->hts/dot_general | solution.py:48
  73.1 5.9 %exponential_bitcast_fusion.2 = f32[4,64,64,128]{3,0,2,1:T(4,128)S(1)} fusion(f32[64,4,128]{2,1,0:T(4,128)S(1)} %fusion.102, pred[64,64]{1,0:T(8,128)(4,1)S(1)} %fusion.104), kind=kLoop, calls=%fused_computation.29.clone.1 | loop fusion | flops 4194304 | bytes 8523776 | tf_op jit(solution)/shard_map/while
  79.9 7.3 %fusion.105 = f32[4,64,64]{1,2,0:T(8,128)S(1)} fusion(f32[4,64,64,128]{3,0,2,1:T(4,128)S(1)} %exponential_bitcast_fusion.2, f32[4,128,64]{1,2,0:T(8,128)S(1)} %copy.154, f32[4,128,64]{1,2,0:T(8,128)S(1)} %copy.155), kind=kLoop, calls=%fused_computation.28.clone.1 | loop fusion | flops 6275072 | bytes 8716288 | tf_op jit(solution)/shard_map/while/body/eval_jaxpr/thk,shk,tshk->hts/dot_general | solution.py:48
  92.2 5.9 %exponential_bitcast_fusion.2 = f32[4,64,64,128]{3,0,2,1:T(4,128)S(1)} fusion(f32[64,4,128]{2,1,0:T(4,128)S(1)} %fusion.102, pred[64,64]{1,0:T(8,128)(4,1)S(1)} %fusion.104), kind=kLoop, calls=%fused_computation.29.clone.1 | loop fusion | flops 4194304 | bytes 8523776 | tf_op jit(solution)/shard_map/while
  99.1 7.3 %fusion.105 = f32[4,64,64]{1,2,0:T(8,128)S(1)} fusion(f32[4,64,64,128]{3,0,2,1:T(4,128)S(1)} %exponential_bitcast_fusion.2, f32[4,128,64]{1,2,0:T(8,128)S(1)} %copy.154, f32[4,128,64]{1,2,0:T(8,128)S(1)} %copy.155), kind=kLoop, calls=%fused_computation.28.clone.1 | loop fusion | flops 6275072 | bytes 8716288 | tf_op jit(solution)/shard_map/while/body/eval_jaxpr/thk,shk,tshk->hts/dot_general | solution.py:48
  111.1 3.4 fusion.43
  124.4 27.6 %all_gather.26 = bf16[16,4,128]{2,1,0:T(4,128)(2,1)S(1)} all-gather(bf16[1,4,128]{2,1,0:T(4,128)(2,1)S(1)} %fusion.69), channel_id=1, replica_groups=mesh['sp'=16,'tp'=2] {'sp'}, dimensions={0}, use_global_device_ids=true | all-gather | bytes 17408 | tf_op jit(solution)/shard_map/all_gather | solution.py:14
  153.5 3.3 fusion.45
  156.9 13.0 %all-gather.12.cloned.1.call-done = bf16[64,128,128]{2,1,0:T(8,128)(2,1)} async-done(((bf16[4,128,128]{2,1,0:T(8,128)(2,1)}), bf16[64,128,128]{2,1,0:T(8,128)(2,1)}) %all-gather.12.cloned.1.call-update) | async-done | bytes 2097168 | tf_op jit(solution)/shard_map/all_gather | solution.py:14
  169.9 18.7 %while.48 = (s32[]{:T(128)}, f32[4,128]{1,0:T(4,128)S(1)}, f32[4,128,128]{2,1,0:T(8,128)S(1)}, s32[]{:T(128)}, bf16[16,4,128]{2,1,0:T(4,128)(2,1)S(1)}, /*index=...) while((s32[]{:T(128)}, f32[4,128]{1,0:T(4,128)S(1)}, f32[4,128,128]{2,1,0:T(8,128)S(1)}, ...), condition=%wide.region_7.8_spmd.clone, body=%wide.region_6.7_spmd.clone.sunk | while | flops 330244 | bytes 665727 | solution.py:27
  190.6 3.4 all_gather.29
  194.8 52.4 %all-gather.8.cloned.1.call-done = bf16[4096,512]{1,0:T(8,128)(2,1)} async-done(((bf16[256,512]{1,0:T(8,128)(2,1)}), bf16[4096,512]{1,0:T(8,128)(2,1)}) %all-gather.8.cloned.1.call-update) | async-done | bytes 4194320 | tf_op jit(solution)/shard_map/all_gather | solution.py:182
  247.1 6.4 %copy.101 = bf16[4096,512]{0,1:T(8,128)(2,1)} copy(bf16[4096,512]{1,0:T(8,128)(2,1)} %all-gather.8.cloned.1.call-done) | data formatting | bytes 8388608 | tf_op jit(solution)/shard_map/while | solution.py:213
  253.5 70.5 %all-gather.10.cloned.1.call-done = bf16[4096,512]{1,0:T(8,128)(2,1)} async-done(((bf16[256,512]{1,0:T(8,128)(2,1)}), bf16[4096,512]{1,0:T(8,128)(2,1)}) %all-gather.10.cloned.1.call-update) | async-done | bytes 4194320 | tf_op jit(solution)/shard_map/all_gather | solution.py:183
  324.0 6.4 %copy.102 = bf16[4096,512]{0,1:T(8,128)(2,1)} copy(bf16[4096,512]{1,0:T(8,128)(2,1)} %all-gather.10.cloned.1.call-done) | data formatting | bytes 8388608 | tf_op jit(solution)/shard_map/while | solution.py:213
  330.4 60.8 %while.46 = (s32[]{:T(128)}, f32[8,256]{1,0:T(8,128)S(1)}, f32[8,256]{1,0:T(8,128)S(1)}, f32[256,8,64]{0,2,1:T(8,128)S(1)}, s32[256]{0:T(256)S(1)}, /*index=5*/b...) while((s32[]{:T(128)}, f32[8,256]{1,0:T(8,128)S(1)}, ...), condition=%wide.region_14.15_spmd, body=%wide.region_9.14_spmd.sunk | while | flops 286661120 | bytes 17810780 | solution.py:213
  331.7 6.3 %conditional.2 = ((f32[8,256]{1,0:T(8,128)S(1)}, f32[8,256]{1,0:T(8,128)S(1)}, f32[256,8,64]{0,2,1:T(8,128)S(1)})) conditional(s32[]{:T(128)} %convert_element_type.161, (f32[8,256]{1,0:T(8,128)S(1)}, f32[8,256]{1,0:T(8,128)S(1)}, f32[256,8,64]{0,2,1:T(8,128)S(1)}) %tuple.108, (s32[]{:T(128)}, s32[512]{0:T(512)S(1)}, s32[256]{0:T(256)S(1)}, ...), branch_computations={%region_10.10_spmd, %region_11.13_spmd} | conditional | flops 286661120 | bytes 17808462 | solution.py:210
  339.3 6.3 %conditional.2 = ((f32[8,256]{1,0:T(8,128)S(1)}, f32[8,256]{1,0:T(8,128)S(1)}, f32[256,8,64]{0,2,1:T(8,128)S(1)})) conditional(s32[]{:T(128)} %convert_element_type.161, (f32[8,256]{1,0:T(8,128)S(1)}, f32[8,256]{1,0:T(8,128)S(1)}, f32[256,8,64]{0,2,1:T(8,128)S(1)}) %tuple.108, (s32[]{:T(128)}, s32[512]{0:T(512)S(1)}, s32[256]{0:T(256)S(1)}, ...), branch_computations={%region_10.10_spmd, %region_11.13_spmd} | conditional | flops 286661120 | bytes 17808462 | solution.py:210
  346.9 6.3 %conditional.2 = ((f32[8,256]{1,0:T(8,128)S(1)}, f32[8,256]{1,0:T(8,128)S(1)}, f32[256,8,64]{0,2,1:T(8,128)S(1)})) conditional(s32[]{:T(128)} %convert_element_type.161, (f32[8,256]{1,0:T(8,128)S(1)}, f32[8,256]{1,0:T(8,128)S(1)}, f32[256,8,64]{0,2,1:T(8,128)S(1)}) %tuple.108, (s32[]{:T(128)}, s32[512]{0:T(512)S(1)}, s32[256]{0:T(256)S(1)}, ...), branch_computations={%region_10.10_spmd, %region_11.13_spmd} | conditional | flops 286661120 | bytes 17808462 | solution.py:210
  354.5 6.3 %conditional.2 = ((f32[8,256]{1,0:T(8,128)S(1)}, f32[8,256]{1,0:T(8,128)S(1)}, f32[256,8,64]{0,2,1:T(8,128)S(1)})) conditional(s32[]{:T(128)} %convert_element_type.161, (f32[8,256]{1,0:T(8,128)S(1)}, f32[8,256]{1,0:T(8,128)S(1)}, f32[256,8,64]{0,2,1:T(8,128)S(1)}) %tuple.108, (s32[]{:T(128)}, s32[512]{0:T(512)S(1)}, s32[256]{0:T(256)S(1)}, ...), branch_computations={%region_10.10_spmd, %region_11.13_spmd} | conditional | flops 286661120 | bytes 17808462 | solution.py:210
  362.1 6.3 %conditional.2 = ((f32[8,256]{1,0:T(8,128)S(1)}, f32[8,256]{1,0:T(8,128)S(1)}, f32[256,8,64]{0,2,1:T(8,128)S(1)})) conditional(s32[]{:T(128)} %convert_element_type.161, (f32[8,256]{1,0:T(8,128)S(1)}, f32[8,256]{1,0:T(8,128)S(1)}, f32[256,8,64]{0,2,1:T(8,128)S(1)}) %tuple.108, (s32[]{:T(128)}, s32[512]{0:T(512)S(1)}, s32[256]{0:T(256)S(1)}, ...), branch_computations={%region_10.10_spmd, %region_11.13_spmd} | conditional | flops 286661120 | bytes 17808462 | solution.py:210
  369.7 6.3 %conditional.2 = ((f32[8,256]{1,0:T(8,128)S(1)}, f32[8,256]{1,0:T(8,128)S(1)}, f32[256,8,64]{0,2,1:T(8,128)S(1)})) conditional(s32[]{:T(128)} %convert_element_type.161, (f32[8,256]{1,0:T(8,128)S(1)}, f32[8,256]{1,0:T(8,128)S(1)}, f32[256,8,64]{0,2,1:T(8,128)S(1)}) %tuple.108, (s32[]{:T(128)}, s32[512]{0:T(512)S(1)}, s32[256]{0:T(256)S(1)}, ...), branch_computations={%region_10.10_spmd, %region_11.13_spmd} | conditional | flops 286661120 | bytes 17808462 | solution.py:210
  377.2 6.3 %conditional.2 = ((f32[8,256]{1,0:T(8,128)S(1)}, f32[8,256]{1,0:T(8,128)S(1)}, f32[256,8,64]{0,2,1:T(8,128)S(1)})) conditional(s32[]{:T(128)} %convert_element_type.161, (f32[8,256]{1,0:T(8,128)S(1)}, f32[8,256]{1,0:T(8,128)S(1)}, f32[256,8,64]{0,2,1:T(8,128)S(1)}) %tuple.108, (s32[]{:T(128)}, s32[512]{0:T(512)S(1)}, s32[256]{0:T(256)S(1)}, ...), branch_computations={%region_10.10_spmd, %region_11.13_spmd} | conditional | flops 286661120 | bytes 17808462 | solution.py:210
  384.8 6.3 %conditional.2 = ((f32[8,256]{1,0:T(8,128)S(1)}, f32[8,256]{1,0:T(8,128)S(1)}, f32[256,8,64]{0,2,1:T(8,128)S(1)})) conditional(s32[]{:T(128)} %convert_element_type.161, (f32[8,256]{1,0:T(8,128)S(1)}, f32[8,256]{1,0:T(8,128)S(1)}, f32[256,8,64]{0,2,1:T(8,128)S(1)}) %tuple.108, (s32[]{:T(128)}, s32[512]{0:T(512)S(1)}, s32[256]{0:T(256)S(1)}, ...), branch_computations={%region_10.10_spmd, %region_11.13_spmd} | conditional | flops 286661120 | bytes 17808462 | solution.py:210
  391.5 3.4 all_gather.32
  (273 shorter events, 124.2 us)
Async XLA Ops:
  6.5 187.5 %copy-start = (bf16[1024,1024]{1,0:T(8,128)(2,1)S(1)}, bf16[1024,1024]{1,0:T(8,128)(2,1)}, u32[]{:S(2)}) copy-start(bf16[1024,1024]{1,0:T(8,128)(2,1)} %param.38) | copy-start | bytes 6291460
  6.5 13.1 %all-gather.6.cloned.1.call-start = ((), (), s32[]{:S(2)}) async-start(), calls=%async_computation | async-start | bytes 1572864 | tf_op jit(solution)/shard_map/all_gather | solution.py:126
  7.3 162.7 %all-gather.12.cloned.1.call-start = ((), (), s32[]{:S(2)}) async-start(), calls=%async_computation.3 | async-start | bytes 2228224 | tf_op jit(solution)/shard_map/all_gather | solution.py:14
  21.1 3.8 copy-start.14
  23.9 3.6 copy-start.4
  31.1 2.7 copy-start.6
  111.0 4.5 %copy-start.7 = (f32[256,512]{1,0:T(8,128)S(1)}, f32[256,512]{1,0:T(8,128)}, u32[]{:S(2)}) copy-start(f32[256,512]{1,0:T(8,128)} %copy-done.6) | copy-start | bytes 1572868
  111.1 136.1 %all-gather.8.cloned.1.call-start = ((), (), s32[]{:S(2)}) async-start(), calls=%async_computation.1 | async-start | bytes 4456448 | tf_op jit(solution)/shard_map/all_gather | solution.py:182
  114.5 4.1 %copy-start.5 = (f32[256,512]{1,0:T(8,128)S(1)}, f32[256,512]{1,0:T(8,128)}, u32[]{:S(2)}) copy-start(f32[256,512]{1,0:T(8,128)} %copy-done.4) | copy-start | bytes 1572868
  114.5 4.1 %copy-start.10 = (f32[256,4]{0,1:T(4,128)S(1)}, f32[256,4]{0,1:T(4,128)}, u32[]{:S(2)}) copy-start(f32[256,4]{0,1:T(4,128)} %param.30) | copy-start | bytes 12292
  114.5 209.5 %all-gather.10.cloned.1.call-start = ((), (), s32[]{:S(2)}) async-start(), calls=%async_computation.2 | async-start | bytes 4456448 | tf_op jit(solution)/shard_map/all_gather | solution.py:183
  119.2 1.2 copy-start.8
  119.2 2.0 copy-start.13
  156.9 31.8 %copy-start.2 = (f32[256,4,128]{0,2,1:T(8,128)S(1)}, f32[256,4,128]{0,2,1:T(8,128)}, u32[]{:S(2)}) copy-start(f32[256,4,128]{0,2,1:T(8,128)} %copy.99) | copy-start | bytes 1572868
  188.7 1.8 copy-start.11
  253.5 76.9 %copy-start.9 = (bf16[256,512]{0,1:T(8,128)(2,1)S(1)}, bf16[256,512]{0,1:T(8,128)(2,1)}, u32[]{:S(2)}) copy-start(bf16[256,512]{0,1:T(8,128)(2,1)} %copy.100) | copy-start | bytes 786436
  330.4 61.0 %copy-start.12 = (f32[512]{0:T(512)S(1)}, f32[512]{0:T(512)}, u32[]{:S(2)}) copy-start(f32[512]{0:T(512)} %param.37) | copy-start | bytes 6148
  391.2 3.7 copy-start.3
  391.5 4.9 %copy-start.1 = (bf16[1024,1024]{1,0:T(8,128)(2,1)S(1)}, bf16[1024,1024]{1,0:T(8,128)(2,1)}, u32[]{:S(2)}) copy-start(bf16[1024,1024]{1,0:T(8,128)(2,1)} %param.38) | copy-start | bytes 6291460
Sparse Core Ops, SparseCore 0:
  8.9 10.6 all-gather.5
  111.2 58.7 all-gather.11
  172.7 74.3 all-gather.7
  249.7 74.1 all-gather.9
where the time goes:
time: 405 us; the launch traced here: 403 us
  waiting for transfers between devices  147 us (36%)
  other arithmetic  99 us (24%)
  local copies, waits for them, and re-layouts  51.6 us (13%)
  matrix products  50 us (12%)
  blocking collectives  34.3 us (8%)
  between operations  13.5 us (3%)
  loops' own time  6.83 us (2%)
    all_gather x1, waiting for transfers between devices, shards(): value_part = lax.all_gather(projected[5], 'sp', axis=0, tiled=True)  70.5 us
    all_gather x1, waiting for transfers between devices, shards(): key_part = lax.all_gather(projected[4], 'sp', axis=0, tiled=True)  52.4 us
    dot_general x4, other arithmetic, advance(): jnp.einsum('thk,shk,tshk->hts', query_block, k_block, jnp.exp(offsets), p...  29.1 us
    all_gather x1, blocking collectives, prefix(): lax.all_gather(part.astype(kind), axis)  27.6 us
    while x4, other arithmetic  23.5 us
    select_n x32, other arithmetic, step(): return jax.tree.map(lambda a, b: jnp.where(reached, a, b), new, before)  18 us
    dot_general x6, matrix products, shards(): jnp.dot(scaled, weight, preferred_element_type=jnp.float32)  16.1 us
    all_gather x1, waiting for transfers between devices, prefix(): lax.all_gather(part.astype(kind), axis)  13 us
  transfers between devices with their start and end apart: 4, of which 4 were waited for; matrix products, arithmetic and copies ran while one was open for 11% of the time, Pallas kernels for 0%

commit v1 on v0

--- a/solution.py
+++ b/solution.py
@@ -180,7 +180,9 @@
         )
     )
     key_part = lax.all_gather(projected[4], "sp", axis=0, tiled=True)
-    value_part = lax.all_gather(projected[5], "sp", axis=0, tiled=True)
+    value_part = jnp.concatenate(
+        lax.all_to_all(jnp.stack([projected[5]] * lax.axis_size("sp")), "sp", 0, 0), axis=0
+    )
     total_amount = key_part.shape[0]
     step_rows = 2 * height
 

time: 405 us -> 426 us (1.052)
  blocking collectives: 34.3 us -> 135 us
  waiting for transfers between devices: 147 us -> 52 us
  local copies, waits for them, and re-layouts: 51.6 us -> 61.6 us
  starting transfers between devices: 0.35 us -> 6.44 us
    all_gather x1, blocking collectives: 27.6 us -> 122 us  [prefix(): lax.all_gather(part.astype(kind), axis)]
    all_gather x1 -> x0, waiting for transfers between devices: 70.5 us -> none  [shards(): value_part = lax.all_gather(projected[5], 'sp', axis=0, tiled=True)]
    all_gather x1, waiting for transfers between devices: 13 us -> 0.02 us  [prefix(): lax.all_gather(part.astype(kind), axis)]
    all_gather x1, waiting for transfers between devices: 52.4 us -> 41.2 us  [shards(): key_part = lax.all_gather(projected[4], 'sp', axis=0, tiled=True)]
    all_to_all x0 -> x1, starting transfers between devices: none -> 6.36 us  [shards(): lax.all_to_all(jnp.stack([projected[5]] * lax.axis_size('sp')), 'sp', 0, 0)]
    all_to_all x0 -> x1, local copies, waits for them, and re-layouts: none -> 6.36 us  [shards(): lax.all_to_all(jnp.stack([projected[5]] * lax.axis_size('sp')), 'sp', 0, 0)]
    all_gather x1, blocking collectives: 3.41 us -> 9.27 us  [shards(): lax.all_gather(rec_rows, 'tp', axis=1, tiled=True)]
  transfers between devices with their start and end apart: 4 -> 4, of which waited for: 4 -> 2; matrix products, arithmetic and copies ran while one was open for 11% -> 13% of each run, Pallas kernels for 0% -> 0%
where the time goes in v1:
time: 426 us; the launch traced here: 424 us
  blocking collectives  135 us (32%)
  other arithmetic  99.7 us (23%)
  local copies, waits for them, and re-layouts  61.6 us (14%)
  waiting for transfers between devices  52 us (12%)
  matrix products  48.7 us (11%)
  between operations  13.5 us (3%)
  loops' own time  7.23 us (2%)
  starting transfers between devices  6.44 us (2%)
    all_gather x1, blocking collectives, prefix(): lax.all_gather(part.astype(kind), axis)  122 us
    all_gather x1, waiting for transfers between devices, shards(): key_part = lax.all_gather(projected[4], 'sp', axis=0, tiled=True)  41.2 us
    dot_general x4, other arithmetic, advance(): jnp.einsum('thk,shk,tshk->hts', query_block, k_block, jnp.exp(offsets), p...  29.1 us
    while x4, other arithmetic  23.5 us
    select_n x32, other arithmetic, step(): return jax.tree.map(lambda a, b: jnp.where(reached, a, b), new, before)  18 us
    dot_general x6, matrix products, shards(): jnp.dot(scaled, weight, preferred_element_type=jnp.float32)  14.8 us
    while x2, local copies, waits for them, and re-layouts, shards(): folded = lax.fori_loop(0, total_amount // step_rows, advance_keys, initial)  12.9 us
    dot_general x8, matrix products, compute(): jnp.einsum('qhd,khd->hqk', group_query, key_rows, preferred_element_type=...  11.5 us
  transfers between devices with their start and end apart: 4, of which 2 were waited for; matrix products, arithmetic and copies ran while one was open for 13% of the time, Pallas kernels for 0%

profile of v1, /device:TPU:29, one launch (start us, length us, event | category | flops | bytes accessed | tf_op | source)
XLA Modules:
  0.0 424.1 jit_solution(243386072216345060)
XLA Ops:
  9.5 10.1 %all-gather.5.cloned.1.call-done = bf16[256,2048]{1,0:T(8,128)(2,1)} async-done(((bf16[256,1024]{1,0:T(8,128)(2,1)}), bf16[256,2048]{1,0:T(8,128)(2,1)}) %all-gather.5.cloned.1.call-update) | async-done | bytes 1048592 | tf_op jit(solution)/shard_map/all_gather | solution.py:126
  21.1 2.7 fusion.51
  28.5 2.7 fusion.46
  33.9 76.8 %while.47 = (s32[]{:T(128)}, f32[4,128,128]{2,1,0:T(8,128)S(1)}, f32[4,64,4,128]{3,1,0,2:T(8,128)}, f32[4,64,4,128]{3,2,1,0:T(4,128)}, f32[4,64,4,128]{3,2,1,0:T...) while((s32[]{:T(128)}, f32[4,128,128]{2,1,0:T(8,128)S(1)}, ...), condition=%wide.region_3.4_spmd.clone, body=%wide.region_1.3_spmd.clone.sunk | while | flops 138760192 | bytes 21254276 | solution.py:66
  34.9 5.9 %exponential_bitcast_fusion.2 = f32[4,64,64,128]{3,0,2,1:T(4,128)S(1)} fusion(f32[64,4,128]{2,1,0:T(4,128)S(1)} %fusion.102, pred[64,64]{1,0:T(8,128)(4,1)S(1)} %fusion.104), kind=kLoop, calls=%fused_computation.29.clone.1 | loop fusion | flops 4194304 | bytes 8523776 | tf_op jit(solution)/shard_map/while
  41.7 7.3 %fusion.105 = f32[4,64,64]{1,2,0:T(8,128)S(1)} fusion(f32[4,64,64,128]{3,0,2,1:T(4,128)S(1)} %exponential_bitcast_fusion.2, f32[4,128,64]{1,2,0:T(8,128)S(1)} %copy.178, f32[4,128,64]{1,2,0:T(8,128)S(1)} %copy.179), kind=kLoop, calls=%fused_computation.28.clone.1 | loop fusion | flops 6275072 | bytes 8716288 | tf_op jit(solution)/shard_map/while/body/eval_jaxpr/thk,shk,tshk->hts/dot_general | solution.py:48
  54.0 5.9 %exponential_bitcast_fusion.2 = f32[4,64,64,128]{3,0,2,1:T(4,128)S(1)} fusion(f32[64,4,128]{2,1,0:T(4,128)S(1)} %fusion.102, pred[64,64]{1,0:T(8,128)(4,1)S(1)} %fusion.104), kind=kLoop, calls=%fused_computation.29.clone.1 | loop fusion | flops 4194304 | bytes 8523776 | tf_op jit(solution)/shard_map/while
  60.8 7.3 %fusion.105 = f32[4,64,64]{1,2,0:T(8,128)S(1)} fusion(f32[4,64,64,128]{3,0,2,1:T(4,128)S(1)} %exponential_bitcast_fusion.2, f32[4,128,64]{1,2,0:T(8,128)S(1)} %copy.178, f32[4,128,64]{1,2,0:T(8,128)S(1)} %copy.179), kind=kLoop, calls=%fused_computation.28.clone.1 | loop fusion | flops 6275072 | bytes 8716288 | tf_op jit(solution)/shard_map/while/body/eval_jaxpr/thk,shk,tshk->hts/dot_general | solution.py:48
  73.1 5.9 %exponential_bitcast_fusion.2 = f32[4,64,64,128]{3,0,2,1:T(4,128)S(1)} fusion(f32[64,4,128]{2,1,0:T(4,128)S(1)} %fusion.102, pred[64,64]{1,0:T(8,128)(4,1)S(1)} %fusion.104), kind=kLoop, calls=%fused_computation.29.clone.1 | loop fusion | flops 4194304 | bytes 8523776 | tf_op jit(solution)/shard_map/while
  80.0 7.3 %fusion.105 = f32[4,64,64]{1,2,0:T(8,128)S(1)} fusion(f32[4,64,64,128]{3,0,2,1:T(4,128)S(1)} %exponential_bitcast_fusion.2, f32[4,128,64]{1,2,0:T(8,128)S(1)} %copy.178, f32[4,128,64]{1,2,0:T(8,128)S(1)} %copy.179), kind=kLoop, calls=%fused_computation.28.clone.1 | loop fusion | flops 6275072 | bytes 8716288 | tf_op jit(solution)/shard_map/while/body/eval_jaxpr/thk,shk,tshk->hts/dot_general | solution.py:48
  92.3 5.9 %exponential_bitcast_fusion.2 = f32[4,64,64,128]{3,0,2,1:T(4,128)S(1)} fusion(f32[64,4,128]{2,1,0:T(4,128)S(1)} %fusion.102, pred[64,64]{1,0:T(8,128)(4,1)S(1)} %fusion.104), kind=kLoop, calls=%fused_computation.29.clone.1 | loop fusion | flops 4194304 | bytes 8523776 | tf_op jit(solution)/shard_map/while
  99.1 7.3 %fusion.105 = f32[4,64,64]{1,2,0:T(8,128)S(1)} fusion(f32[4,64,64,128]{3,0,2,1:T(4,128)S(1)} %exponential_bitcast_fusion.2, f32[4,128,64]{1,2,0:T(8,128)S(1)} %copy.178, f32[4,128,64]{1,2,0:T(8,128)S(1)} %copy.179), kind=kLoop, calls=%fused_computation.28.clone.1 | loop fusion | flops 6275072 | bytes 8716288 | tf_op jit(solution)/shard_map/while/body/eval_jaxpr/thk,shk,tshk->hts/dot_general | solution.py:48
  120.5 2.7 fusion.45
  125.7 6.4 %all-to-all-start = ((bf16[16,256,512]{1,2,0:T(8,128)(2,1)}), bf16[16,256,512]{1,2,0:T(8,128)(2,1)}, u32[]{:S(2)}, u32[]{:S(2)}) async-start(bf16[16,256,512]{1,2,0:T(8,128)(2,1)} %stack.2), calls=%async_computation | async-start | bytes 8388608 | tf_op jit(solution)/shard_map/all_to_all | solution.py:184
  132.8 122.3 %all_gather.23 = bf16[16,4,128]{2,1,0:T(4,128)(2,1)S(1)} all-gather(bf16[1,4,128]{2,1,0:T(4,128)(2,1)S(1)} %fusion.69), channel_id=1, replica_groups=mesh['sp'=16,'tp'=2] {'sp'}, dimensions={0}, use_global_device_ids=true | all-gather | bytes 17408 | tf_op jit(solution)/shard_map/all_gather | solution.py:14
  256.6 3.3 fusion.43
  260.0 18.8 %while.48 = (s32[]{:T(128)}, f32[4,128]{1,0:T(4,128)S(1)}, f32[4,128,128]{2,1,0:T(8,128)S(1)}, s32[]{:T(128)}, bf16[16,4,128]{2,1,0:T(4,128)(2,1)S(1)}, /*index=...) while((s32[]{:T(128)}, f32[4,128]{1,0:T(4,128)S(1)}, f32[4,128,128]{2,1,0:T(8,128)S(1)}, ...), condition=%wide.region_7.8_spmd.clone, body=%wide.region_6.7_spmd.clone.sunk | while | flops 330244 | bytes 665727 | solution.py:27
  280.8 9.3 %all_gather.26 = bf16[256,1024]{0,1:T(8,128)(2,1)S(1)} all-gather(bf16[256,512]{0,1:T(8,128)(2,1)S(1)} %fusion.56), channel_id=1, replica_groups=mesh['sp'=16,'tp'=2] {'tp'}, dimensions={1}, use_global_device_ids=true | all-gather | bytes 786432 | tf_op jit(solution)/shard_map/all_gather | solution.py:222
  290.8 6.4 %copy.124 = bf16[16,256,512]{2,1,0:T(8,128)(2,1)} copy(bf16[16,256,512]{1,2,0:T(8,128)(2,1)} %all-to-all-done) | data formatting | bytes 8388608 | tf_op jit(solution)/shard_map/all_to_all | solution.py:184
  297.1 6.5 %copy.126 = bf16[4096,512]{0,1:T(8,128)(2,1)} copy(bf16[4096,512]{1,0:T(8,128)(2,1)} %bitcast.180) | data formatting | bytes 8388608 | tf_op jit(solution)/shard_map/while | solution.py:215
  303.6 41.2 %all-gather.7.cloned.1.call-done = bf16[4096,512]{1,0:T(8,128)(2,1)} async-done(((bf16[256,512]{1,0:T(8,128)(2,1)}), bf16[4096,512]{1,0:T(8,128)(2,1)}) %all-gather.7.cloned.1.call-update) | async-done | bytes 4194320 | tf_op jit(solution)/shard_map/all_gather | solution.py:182
  344.8 6.4 %copy.125 = bf16[4096,512]{0,1:T(8,128)(2,1)} copy(bf16[4096,512]{1,0:T(8,128)(2,1)} %all-gather.7.cloned.1.call-done) | data formatting | bytes 8388608 | tf_op jit(solution)/shard_map/while | solution.py:215
  351.3 61.1 %while.46 = (s32[]{:T(128)}, f32[8,256]{1,0:T(8,128)S(1)}, f32[8,256]{1,0:T(8,128)S(1)}, f32[256,8,64]{0,2,1:T(8,128)S(1)}, s32[256]{0:T(256)S(1)}, /*index=5*/b...) while((s32[]{:T(128)}, f32[8,256]{1,0:T(8,128)S(1)}, ...), condition=%wide.region_14.15_spmd, body=%wide.region_9.14_spmd.sunk | while | flops 286661120 | bytes 17810780 | solution.py:215
  352.5 6.4 %conditional.2 = ((f32[8,256]{1,0:T(8,128)S(1)}, f32[8,256]{1,0:T(8,128)S(1)}, f32[256,8,64]{0,2,1:T(8,128)S(1)})) conditional(s32[]{:T(128)} %convert_element_type.161, (f32[8,256]{1,0:T(8,128)S(1)}, f32[8,256]{1,0:T(8,128)S(1)}, f32[256,8,64]{0,2,1:T(8,128)S(1)}) %tuple.110, (s32[]{:T(128)}, s32[512]{0:T(512)S(1)}, s32[256]{0:T(256)S(1)}, ...), branch_computations={%region_10.10_spmd, %region_11.13_spmd} | conditional | flops 286661120 | bytes 17808462 | solution.py:212
  360.2 6.4 %conditional.2 = ((f32[8,256]{1,0:T(8,128)S(1)}, f32[8,256]{1,0:T(8,128)S(1)}, f32[256,8,64]{0,2,1:T(8,128)S(1)})) conditional(s32[]{:T(128)} %convert_element_type.161, (f32[8,256]{1,0:T(8,128)S(1)}, f32[8,256]{1,0:T(8,128)S(1)}, f32[256,8,64]{0,2,1:T(8,128)S(1)}) %tuple.110, (s32[]{:T(128)}, s32[512]{0:T(512)S(1)}, s32[256]{0:T(256)S(1)}, ...), branch_computations={%region_10.10_spmd, %region_11.13_spmd} | conditional | flops 286661120 | bytes 17808462 | solution.py:212
  367.8 6.4 %conditional.2 = ((f32[8,256]{1,0:T(8,128)S(1)}, f32[8,256]{1,0:T(8,128)S(1)}, f32[256,8,64]{0,2,1:T(8,128)S(1)})) conditional(s32[]{:T(128)} %convert_element_type.161, (f32[8,256]{1,0:T(8,128)S(1)}, f32[8,256]{1,0:T(8,128)S(1)}, f32[256,8,64]{0,2,1:T(8,128)S(1)}) %tuple.110, (s32[]{:T(128)}, s32[512]{0:T(512)S(1)}, s32[256]{0:T(256)S(1)}, ...), branch_computations={%region_10.10_spmd, %region_11.13_spmd} | conditional | flops 286661120 | bytes 17808462 | solution.py:212
  375.5 6.4 %conditional.2 = ((f32[8,256]{1,0:T(8,128)S(1)}, f32[8,256]{1,0:T(8,128)S(1)}, f32[256,8,64]{0,2,1:T(8,128)S(1)})) conditional(s32[]{:T(128)} %convert_element_type.161, (f32[8,256]{1,0:T(8,128)S(1)}, f32[8,256]{1,0:T(8,128)S(1)}, f32[256,8,64]{0,2,1:T(8,128)S(1)}) %tuple.110, (s32[]{:T(128)}, s32[512]{0:T(512)S(1)}, s32[256]{0:T(256)S(1)}, ...), branch_computations={%region_10.10_spmd, %region_11.13_spmd} | conditional | flops 286661120 | bytes 17808462 | solution.py:212
  383.1 6.4 %conditional.2 = ((f32[8,256]{1,0:T(8,128)S(1)}, f32[8,256]{1,0:T(8,128)S(1)}, f32[256,8,64]{0,2,1:T(8,128)S(1)})) conditional(s32[]{:T(128)} %convert_element_type.161, (f32[8,256]{1,0:T(8,128)S(1)}, f32[8,256]{1,0:T(8,128)S(1)}, f32[256,8,64]{0,2,1:T(8,128)S(1)}) %tuple.110, (s32[]{:T(128)}, s32[512]{0:T(512)S(1)}, s32[256]{0:T(256)S(1)}, ...), branch_computations={%region_10.10_spmd, %region_11.13_spmd} | conditional | flops 286661120 | bytes 17808462 | solution.py:212
  390.7 6.4 %conditional.2 = ((f32[8,256]{1,0:T(8,128)S(1)}, f32[8,256]{1,0:T(8,128)S(1)}, f32[256,8,64]{0,2,1:T(8,128)S(1)})) conditional(s32[]{:T(128)} %convert_element_type.161, (f32[8,256]{1,0:T(8,128)S(1)}, f32[8,256]{1,0:T(8,128)S(1)}, f32[256,8,64]{0,2,1:T(8,128)S(1)}) %tuple.110, (s32[]{:T(128)}, s32[512]{0:T(512)S(1)}, s32[256]{0:T(256)S(1)}, ...), branch_computations={%region_10.10_spmd, %region_11.13_spmd} | conditional | flops 286661120 | bytes 17808462 | solution.py:212
  398.4 6.4 %conditional.2 = ((f32[8,256]{1,0:T(8,128)S(1)}, f32[8,256]{1,0:T(8,128)S(1)}, f32[256,8,64]{0,2,1:T(8,128)S(1)})) conditional(s32[]{:T(128)} %convert_element_type.161, (f32[8,256]{1,0:T(8,128)S(1)}, f32[8,256]{1,0:T(8,128)S(1)}, f32[256,8,64]{0,2,1:T(8,128)S(1)}) %tuple.110, (s32[]{:T(128)}, s32[512]{0:T(512)S(1)}, s32[256]{0:T(256)S(1)}, ...), branch_computations={%region_10.10_spmd, %region_11.13_spmd} | conditional | flops 286661120 | bytes 17808462 | solution.py:212
  406.0 6.4 %conditional.2 = ((f32[8,256]{1,0:T(8,128)S(1)}, f32[8,256]{1,0:T(8,128)S(1)}, f32[256,8,64]{0,2,1:T(8,128)S(1)})) conditional(s32[]{:T(128)} %convert_element_type.161, (f32[8,256]{1,0:T(8,128)S(1)}, f32[8,256]{1,0:T(8,128)S(1)}, f32[256,8,64]{0,2,1:T(8,128)S(1)}) %tuple.110, (s32[]{:T(128)}, s32[512]{0:T(512)S(1)}, s32[256]{0:T(256)S(1)}, ...), branch_computations={%region_10.10_spmd, %region_11.13_spmd} | conditional | flops 286661120 | bytes 17808462 | solution.py:212
  412.7 3.4 all_gather.28
  (275 shorter events, 127.6 us)
Async XLA Ops:
  6.5 283.5 %copy-start = (bf16[1024,1024]{1,0:T(8,128)(2,1)S(1)}, bf16[1024,1024]{1,0:T(8,128)(2,1)}, u32[]{:S(2)}) copy-start(bf16[1024,1024]{1,0:T(8,128)(2,1)} %param.38) | copy-start | bytes 6291460
  6.5 13.1 %all-gather.5.cloned.1.call-start = ((), (), s32[]{:S(2)}) async-start(), calls=%async_computation.1 | async-start | bytes 1572864 | tf_op jit(solution)/shard_map/all_gather | solution.py:126
  7.3 252.8 %all-gather.9.cloned.1.call-start = ((), (), s32[]{:S(2)}) async-start(), calls=%async_computation.3 | async-start | bytes 2228224 | tf_op jit(solution)/shard_map/all_gather | solution.py:14
  21.1 3.8 copy-start.14
  23.9 3.7 copy-start.4
  28.5 2.9 copy-start.8
  31.2 2.7 copy-start.6
  110.6 5.5 %copy-start.5 = (f32[256,512]{1,0:T(8,128)S(1)}, f32[256,512]{1,0:T(8,128)}, u32[]{:S(2)}) copy-start(f32[256,512]{1,0:T(8,128)} %copy-done.4) | copy-start | bytes 1572868
  110.7 5.5 %copy-start.10 = (f32[256,4]{0,1:T(4,128)S(1)}, f32[256,4]{0,1:T(4,128)}, u32[]{:S(2)}) copy-start(f32[256,4]{0,1:T(4,128)} %param.30) | copy-start | bytes 12292
  116.8 1.3 copy-start.7
  116.8 2.1 copy-start.13
  125.7 165.1 %all-to-all-start = ((bf16[16,256,512]{1,2,0:T(8,128)(2,1)}), bf16[16,256,512]{1,2,0:T(8,128)(2,1)}, u32[]{:S(2)}, u32[]{:S(2)}) async-start(bf16[16,256,512]{1,2,0:T(8,128)(2,1)} %stack.2), calls=%async_computation | async-start | bytes 8388608 | tf_op jit(solution)/shard_map/all_to_all | solution.py:184
  132.1 212.7 %all-gather.7.cloned.1.call-start = ((), (), s32[]{:S(2)}) async-start(), calls=%async_computation.2 | async-start | bytes 4456448 | tf_op jit(solution)/shard_map/all_gather | solution.py:182
  260.0 18.9 %copy-start.2 = (f32[256,4,128]{0,2,1:T(8,128)S(1)}, f32[256,4,128]{0,2,1:T(8,128)}, u32[]{:S(2)}) copy-start(f32[256,4,128]{0,2,1:T(8,128)} %copy.121) | copy-start | bytes 1572868
  278.8 1.8 copy-start.11
  303.6 47.6 %copy-start.9 = (bf16[256,512]{0,1:T(8,128)(2,1)S(1)}, bf16[256,512]{0,1:T(8,128)(2,1)}, u32[]{:S(2)}) copy-start(bf16[256,512]{0,1:T(8,128)(2,1)} %copy.122) | copy-start | bytes 786436
  351.2 61.3 %copy-start.12 = (f32[512]{0:T(512)S(1)}, f32[512]{0:T(512)}, u32[]{:S(2)}) copy-start(f32[512]{0:T(512)} %param.37) | copy-start | bytes 6148
  412.4 3.7 copy-start.3
  412.7 4.9 %copy-start.1 = (bf16[1024,1024]{1,0:T(8,128)(2,1)S(1)}, bf16[1024,1024]{1,0:T(8,128)(2,1)}, u32[]{:S(2)}) copy-start(bf16[1024,1024]{1,0:T(8,128)(2,1)} %param.38) | copy-start | bytes 6291460
Sparse Core Ops, SparseCore 0:
  8.9 10.6 all-gather.4
  111.5 108.8 all-gather.8
  260.1 84.6 all-gather.6
